TPU v7x, 32 devices: a whole 2x2x4 slice. The times are simulated.
32 devices in a mesh: sp: 8 (over z, y), tp: 4 (over x, core).
Axes of the slice: x: 2, y: 2, z: 4, core: 2. Of those that a mesh axis runs over, the one named last changes fastest.
Arguments:
- stream: bfloat16 [4096, 2048], P('sp', 'tp'), may hold values from -6 to 6
- doc_ids: int32 [4096], P('sp'), may hold values from 0 to 3, never falling along the last dimension, each value on 1 to 2304 neighbouring positions
- norm_gain: float32 [2, 2048], replicated, may hold values from 0.1 to 1.9
- gate_proj: bfloat16 [2, 2048, 2048], P(None, 'sp', 'tp'), may hold values from -0.125 to 0.125
- input_gate: bfloat16 [2, 2048, 2048], P(None, 'sp', 'tp'), may hold values from -0.125 to 0.125
- value_proj: bfloat16 [2, 2048, 2048], P(None, 'sp', 'tp'), may hold values from -0.125 to 0.125
- taps: float32 [2, 3, 2048], P(None, None, 'tp'), may hold values from -3 to 3
- out_proj: bfloat16 [2, 2048, 2048], P(None, 'tp', 'sp'), may hold values from -0.125 to 0.125
Outputs:
- result: bfloat16 [4096, 2048], P('sp', 'tp')
Inputs may be any that keep to these rules, and one draw needn't show every extreme that they name: `doc_ids`: document numbers never fall along the sequence; each document holds 1 to 2304 positions.
All inputs are finite; a program needn't handle non-finite values.
Results may differ from a plain program's by a relative error of at most 0.03.
Values may be sent and summed in bfloat16 or wider, within the bound.
A program may use at most 64 MiB of HBM per device.

v0:
```python
import jax
import jax.numpy as jnp
from jax import lax
from jax.sharding import PartitionSpec as P

epsilon = 1e-06


def with_halo(value, sides, width):
    for axis, dim in sides:
        size, length = (lax.axis_size(axis), value.shape[dim])
        up = [(i, (i + 1) % size) for i in range(size - 1)]
        down = [(j, i) for i, j in up]
        last = lax.slice_in_dim(value, length - width, length, axis=dim)
        leading = lax.slice_in_dim(value, 0, width, axis=dim)
        before = lax.ppermute(last, axis, up)
        after = lax.ppermute(leading, axis, down)
        value = jnp.concatenate([before, value, after], axis=dim)
    return value


def per_device(stream, doc_ids, norm_gain, gate_proj, input_gate, value_proj, taps, out_proj):
    layers = gate_proj.shape[0]
    gathered_in = (
        lax.all_gather(gate_proj, "sp", axis=1, tiled=True),
        lax.all_gather(input_gate, "sp", axis=1, tiled=True),
        lax.all_gather(value_proj, "sp", axis=1, tiled=True),
    )
    gathered_out = lax.all_gather(out_proj, "sp", axis=2, tiled=True)
    current = stream
    for layer_index in range(layers):
        full_rows = lax.all_gather(current, "tp", axis=1, tiled=True)
        widened = full_rows.astype(jnp.float32)
        scale = lax.rsqrt(jnp.mean(widened * widened, axis=-1, keepdims=True) + epsilon)
        normed = (widened * scale * norm_gain[layer_index]).astype(jnp.bfloat16)
        gate_b = jnp.dot(normed, gathered_in[0][layer_index], preferred_element_type=jnp.float32)
        gate_c = jnp.dot(normed, gathered_in[1][layer_index], preferred_element_type=jnp.float32)
        values = jnp.dot(normed, gathered_in[2][layer_index], preferred_element_type=jnp.float32)
        gate_b = gate_b.astype(jnp.bfloat16)
        gate_c = gate_c.astype(jnp.bfloat16)
        values = values.astype(jnp.bfloat16)
        mixed_in = (gate_c.astype(jnp.float32) * values.astype(jnp.float32)).astype(jnp.bfloat16)
        padded, doc_padded = (
            with_halo(mixed_in, (("sp", 0),), 1),
            with_halo(doc_ids, (("sp", 0),), 1),
        )
        same_prev = (doc_padded[:-2] == doc_ids)[:, None]
        same_next = (doc_padded[2:] == doc_ids)[:, None]
        kernel_taps = taps[layer_index]
        convolved = (
            jnp.where(same_prev, kernel_taps[0] * padded[:-2].astype(jnp.float32), 0.0)
            + kernel_taps[1] * mixed_in.astype(jnp.float32)
            + jnp.where(same_next, kernel_taps[2] * padded[2:].astype(jnp.float32), 0.0)
        )
        gated = (gate_b.astype(jnp.float32) * convolved).astype(jnp.bfloat16)
        partials = jnp.dot(gated, gathered_out[layer_index], preferred_element_type=jnp.float32)
        summed = lax.psum_scatter(
            partials.astype(jnp.bfloat16), "tp", scatter_dimension=1, tiled=True
        ).astype(jnp.float32)
        current = (current.astype(jnp.float32) + summed).astype(jnp.bfloat16)
    return current


def solution(mesh):
    in_specs = (
        P("sp", "tp"),
        P("sp"),
        P(),
        P(None, "sp", "tp"),
        P(None, "sp", "tp"),
        P(None, "sp", "tp"),
        P(None, None, "tp"),
        P(None, "tp", "sp"),
    )
    out_specs = P("sp", "tp")
    return jax.shard_map(
        per_device, mesh=mesh, in_specs=in_specs, out_specs=out_specs, check_vma=False
    )
```

profile of v0, /device:TPU:0, one launch (start us, length us, event | category | flops | bytes accessed | tf_op | source)
XLA Modules:
  0.0 454.6 jit_solution(15519410524372381653)
XLA Ops:
  6.5 0.0 all-gather.7.cloned.1.call-start
  6.5 0.7 all-gather.7.cloned.1.call-update
  7.3 0.0 all-gather.13.cloned.1.call-start
  7.3 0.7 all-gather.13.cloned.1.call-update
  8.0 0.0 all-gather.11.cloned.1.call-start
  8.1 0.7 all-gather.11.cloned.1.call-update
  8.7 0.0 all-gather.9.cloned.1.call-start
  8.8 0.5 all-gather.9.cloned.1.call-update
  9.3 0.0 all-gather.15.cloned.1.call-start
  9.4 0.5 all-gather.15.cloned.1.call-update
  9.9 0.0 reduce-scatter.3.cloned.1.call-start
  9.9 1.3 fusion.64
  11.3 5.4 %collective-permute-start = (s32[1]{0:T(128)}, s32[1]{0:T(128)}, u32[]{:S(2)}, u32[]{:S(2)}) collective-permute-start(s32[1]{0:T(128)} %get-tuple-element.21), channel_id=1, source_target_pairs={{0,4},{4,8},{8,12},{12,16},{16,20},{20,24},{24,28},{1,5},{5,9},{9,... | collective-permute-start | bytes 20 | tf_op jit(solution)/shard_map/ppermute | solution.py:16
  16.7 1.3 collective-permute-start.2
  18.0 0.8 fusion.63
  18.8 0.8 fusion.62
  19.6 0.0 collective-permute-done
  19.6 2.5 collective-permute-done.2
  22.2 2.1 pad_add_fusion
  24.3 9.9 %all-gather.7.cloned.1.call-done = bf16[512,2048]{1,0:T(8,128)(2,1)} async-done(((bf16[512,512]{1,0:T(8,128)(2,1)}), bf16[512,2048]{1,0:T(8,128)(2,1)}) %all-gather.7.cloned.1.call-update) | async-done | bytes 2097168 | tf_op jit(solution)/shard_map/all_gather | solution.py:32
  34.2 2.1 fusion
  36.3 72.9 %all-gather.13.cloned.1.call-done = bf16[2,2048,512]{2,1,0:T(8,128)(2,1)} async-done(((bf16[2,256,512]{2,1,0:T(8,128)(2,1)}), bf16[2,2048,512]{2,1,0:T(8,128)(2,1)}) %all-gather.13.cloned.1.call-update) | async-done | bytes 4194320 | tf_op jit(solution)/shard_map/all_gather | solution.py:27
  109.2 0.0 copy-start.2
  109.2 4.7 %fusion.19 = f32[512,512]{1,0:T(8,128)} fusion(bf16[2,2048,512]{2,1,0:T(8,128)(2,1)} %all-gather.13.cloned.1.call-done, bf16[512,2048]{1,0:T(8,128)(2,1)} %all-gather.7.cloned.1.call-done, f32[2048]{0:T(1024)S(1)} %bitcast.79, f32[512]{0:T(512)S(1)} %add_rsqrt_fusion.1), kind=kOutput, calls=%fused_computation.33 | convolution fusion | flops 1078460416 | bytes 5253120 | tf_op jit(solution)/shard_map/dot_general | solution.py:38
  113.9 0.0 copy-start.4
  113.9 68.9 %all-gather.11.cloned.1.call-done = bf16[2,2048,512]{2,1,0:T(8,128)(2,1)} async-done(((bf16[2,256,512]{2,1,0:T(8,128)(2,1)}), bf16[2,2048,512]{2,1,0:T(8,128)(2,1)}) %all-gather.11.cloned.1.call-update) | async-done | bytes 4194320 | tf_op jit(solution)/shard_map/all_gather | solution.py:26
  182.7 0.0 copy-done.2
  182.7 3.1 fusion.30
  185.9 2.5 collective-permute-start.1
  188.4 1.3 collective-permute-start.3
  189.7 0.0 copy-done.4
  189.7 0.1 slice_compare_fusion.1
  189.8 66.4 %all-gather.9.cloned.1.call-done = bf16[2,2048,512]{2,1,0:T(8,128)(2,1)} async-done(((bf16[2,256,512]{2,1,0:T(8,128)(2,1)}), bf16[2,2048,512]{2,1,0:T(8,128)(2,1)}) %all-gather.9.cloned.1.call-update) | async-done | bytes 4194320 | tf_op jit(solution)/shard_map/all_gather | solution.py:25
  256.1 75.1 %all-gather.15.cloned.1.call-done = bf16[2,512,2048]{2,1,0:T(8,128)(2,1)} async-done(((bf16[2,512,256]{2,1,0:T(8,128)(2,1)}), bf16[2,512,2048]{2,1,0:T(8,128)(2,1)}) %all-gather.15.cloned.1.call-update) | async-done | bytes 4194320 | tf_op jit(solution)/shard_map/all_gather | solution.py:29
  331.2 0.0 collective-permute-done.1
  331.2 0.0 collective-permute-done.3
  331.2 0.0 copy-start.1
  331.2 6.3 %convolution_convert_fusion.1 = bf16[512,2048]{1,0:T(8,128)(2,1)} fusion(bf16[2,512,2048]{2,1,0:T(8,128)(2,1)} %all-gather.15.cloned.1.call-done, bf16[2,2048,512]{2,1,0:T(8,128)(2,1)} %all-gather.9.cloned.1.call-done, bf16[512,512]{1,0:T(8,128)(2,1)S(1)} %fusion.30, bf16[1,512]{1,0:T(2,128)(2,1)S(1)} %collective-permute-done.3, ...), kind=kOutput, calls=%fused_computation.11 | convolution fusion | flops 2157969408 | bytes 8932352 | tf_op jit(solution)/shard_map/dot_general | solution.py:56
  337.5 0.0 reduce-scatter.3.cloned.1.call-update
  337.6 0.0 all-gather.17.cloned.1.call-start
  337.6 29.4 %reduce-scatter.3.cloned.1.call-done = bf16[512,512]{1,0:T(8,128)(2,1)} async-done(((bf16[512,2048]{1,0:T(8,128)(2,1)}), bf16[512,512]{1,0:T(8,128)(2,1)}) %reduce-scatter.3.cloned.1.call-update) | async-done | bytes 524304 | tf_op jit(solution)/shard_map/reduce_scatter | solution.py:57
  367.0 0.0 copy-done.1
  367.1 2.0 add_convert_fusion.1
  369.0 0.0 all-gather.17.cloned.1.call-update
  369.0 0.0 reduce-scatter.5.cloned.1.call-start
  369.1 22.7 %all-gather.17.cloned.1.call-done = bf16[512,2048]{1,0:T(8,128)(2,1)} async-done(((bf16[512,512]{1,0:T(8,128)(2,1)}), bf16[512,2048]{1,0:T(8,128)(2,1)}) %all-gather.17.cloned.1.call-update) | async-done | bytes 2097168 | tf_op jit(solution)/shard_map/all_gather | solution.py:32
  391.8 2.1 fusion.3
  393.8 0.0 copy-start.3
  393.8 0.0 copy-start.5
  393.9 3.7 fusion.27
  397.5 0.0 copy-done.3
  397.5 0.4 copy-done.5
  397.9 1.3 fusion.28
  399.2 3.4 collective-permute-start.4
  402.6 1.3 collective-permute-start.5
  403.9 0.0 collective-permute-done.4
  403.9 4.2 collective-permute-done.5
  408.1 0.0 copy-start
  408.1 6.3 %convolution_convert_fusion = bf16[512,2048]{1,0:T(8,128)(2,1)} fusion(bf16[2,512,2048]{2,1,0:T(8,128)(2,1)} %all-gather.15.cloned.1.call-done, bf16[2,2048,512]{2,1,0:T(8,128)(2,1)} %all-gather.9.cloned.1.call-done, bf16[512,512]{1,0:T(8,128)(2,1)S(1)} %fusion.28, bf16[1,512]{1,0:T(2,128)(2,1)S(1)} %collective-permute-done.5, ...), kind=kOutput, calls=%fused_computation.10 | convolution fusion | flops 2157969408 | bytes 8932352 | tf_op jit(solution)/shard_map/dot_general | solution.py:56
  414.4 0.0 reduce-scatter.5.cloned.1.call-update
  414.5 31.3 %reduce-scatter.5.cloned.1.call-done = bf16[512,512]{1,0:T(8,128)(2,1)} async-done(((bf16[512,2048]{1,0:T(8,128)(2,1)}), bf16[512,512]{1,0:T(8,128)(2,1)}) %reduce-scatter.5.cloned.1.call-update) | async-done | bytes 524304 | tf_op jit(solution)/shard_map/reduce_scatter | solution.py:57
  445.8 0.0 copy-done
  445.8 2.0 add_convert_fusion
  (4 shorter events, 0.0 us)
Async XLA Ops:
  6.5 27.7 %all-gather.7.cloned.1.call-start = ((), (), s32[]{:S(2)}) async-start(), calls=%async_computation.2 | async-start | bytes 2621440 | tf_op jit(solution)/shard_map/all_gather | solution.py:32
  7.3 101.9 %all-gather.13.cloned.1.call-start = ((), (), s32[]{:S(2)}) async-start(), calls=%async_computation.5 | async-start | bytes 4718592 | tf_op jit(solution)/shard_map/all_gather | solution.py:27
  8.0 174.7 %all-gather.11.cloned.1.call-start = ((), (), s32[]{:S(2)}) async-start(), calls=%async_computation.4 | async-start | bytes 4718592 | tf_op jit(solution)/shard_map/all_gather | solution.py:26
  8.7 247.4 %all-gather.9.cloned.1.call-start = ((), (), s32[]{:S(2)}) async-start(), calls=%async_computation.3 | async-start | bytes 4718592 | tf_op jit(solution)/shard_map/all_gather | solution.py:25
  9.3 321.9 %all-gather.15.cloned.1.call-start = ((), (), s32[]{:S(2)}) async-start(), calls=%async_computation.6 | async-start | bytes 4718592 | tf_op jit(solution)/shard_map/all_gather | solution.py:29
  9.9 357.1 %reduce-scatter.3.cloned.1.call-start = ((), (), s32[]{:S(2)}) async-start(), calls=%async_computation.7 | async-start | bytes 2621440 | tf_op jit(solution)/shard_map/reduce_scatter | solution.py:57
  11.3 8.3 %collective-permute-start = (s32[1]{0:T(128)}, s32[1]{0:T(128)}, u32[]{:S(2)}, u32[]{:S(2)}) collective-permute-start(s32[1]{0:T(128)} %get-tuple-element.21), channel_id=1, source_target_pairs={{0,4},{4,8},{8,12},{12,16},{16,20},{20,24},{24,28},{1,5},{5,9},{9,... | collective-permute-start | bytes 20 | tf_op jit(solution)/shard_map/ppermute | solution.py:16
  16.7 5.5 %collective-permute-start.2 = (s32[1]{0:T(128)}, s32[1]{0:T(128)}, u32[]{:S(2)}, u32[]{:S(2)}) collective-permute-start(s32[1]{0:T(128)} %get-tuple-element.22), channel_id=1, source_target_pairs={{4,0},{8,4},{12,8},{16,12},{20,16},{24,20},{28,24},{5,1},{9,5},{13... | collective-permute-start | bytes 20 | tf_op jit(solution)/shard_map/ppermute | solution.py:17
  109.2 73.5 %copy-start.2 = (bf16[512,2048]{1,0:T(8,128)(2,1)S(1)}, bf16[512,2048]{1,0:T(8,128)(2,1)}, u32[]{:S(2)}) copy-start(bf16[512,2048]{1,0:T(8,128)(2,1)} %all-gather.7.cloned.1.call-done) | copy-start | bytes 6291460
  113.9 75.8 %copy-start.4 = (s32[512]{0:T(512)S(1)}, s32[512]{0:T(512)}, u32[]{:S(2)}) copy-start(s32[512]{0:T(512)} %param.9) | copy-start | bytes 6148
  185.9 145.3 %collective-permute-start.1 = (bf16[1,512]{1,0:T(2,128)(2,1)S(1)}, bf16[1,512]{1,0:T(2,128)(2,1)S(1)}, u32[]{:S(2)}, u32[]{:S(2)}) collective-permute-start(bf16[1,512]{1,0:T(2,128)(2,1)S(1)} %get-tuple-element.7), channel_id=1, source_target_pairs={{0,4},{4,8},{8,12},{12,16},{16,20},{20,24},{24,28},{1,5},{5,9},{9,... | collective-permute-start | bytes 3080 | tf_op jit(solution)/shard_map/ppermute | solution.py:16
  188.4 142.8 %collective-permute-start.3 = (bf16[1,512]{1,0:T(2,128)(2,1)S(1)}, bf16[1,512]{1,0:T(2,128)(2,1)S(1)}, u32[]{:S(2)}, u32[]{:S(2)}) collective-permute-start(bf16[1,512]{1,0:T(2,128)(2,1)S(1)} %get-tuple-element.8), channel_id=1, source_target_pairs={{4,0},{8,4},{12,8},{16,12},{20,16},{24,20},{28,24},{5,1},{9,5},{13... | collective-permute-start | bytes 3080 | tf_op jit(solution)/shard_map/ppermute | solution.py:17
  331.2 35.8 %copy-start.1 = (bf16[512,512]{1,0:T(8,128)(2,1)S(1)}, bf16[512,512]{1,0:T(8,128)(2,1)}, u32[]{:S(2)}) copy-start(bf16[512,512]{1,0:T(8,128)(2,1)} %param.8) | copy-start | bytes 1572868
  337.6 54.2 %all-gather.17.cloned.1.call-start = ((), (), s32[]{:S(2)}) async-start(), calls=%async_computation.8 | async-start | bytes 2621440 | tf_op jit(solution)/shard_map/all_gather | solution.py:32
  369.0 76.7 %reduce-scatter.5.cloned.1.call-start = ((), (), s32[]{:S(2)}) async-start(), calls=%async_computation.9 | async-start | bytes 2621440 | tf_op jit(solution)/shard_map/reduce_scatter | solution.py:57
  393.8 3.7 copy-start.3
  393.8 4.1 copy-start.5
  399.2 4.7 %collective-permute-start.4 = (bf16[1,512]{1,0:T(2,128)(2,1)S(1)}, bf16[1,512]{1,0:T(2,128)(2,1)S(1)}, u32[]{:S(2)}, u32[]{:S(2)}) collective-permute-start(bf16[1,512]{1,0:T(2,128)(2,1)S(1)} %get-tuple-element.5), channel_id=1, source_target_pairs={{0,4},{4,8},{8,12},{12,16},{16,20},{20,24},{24,28},{1,5},{5,9},{9,... | collective-permute-start | bytes 3080 | tf_op jit(solution)/shard_map/ppermute | solution.py:16
  402.6 5.5 %collective-permute-start.5 = (bf16[1,512]{1,0:T(2,128)(2,1)S(1)}, bf16[1,512]{1,0:T(2,128)(2,1)S(1)}, u32[]{:S(2)}, u32[]{:S(2)}) collective-permute-start(bf16[1,512]{1,0:T(2,128)(2,1)S(1)} %get-tuple-element.6), channel_id=1, source_target_pairs={{4,0},{8,4},{12,8},{16,12},{20,16},{24,20},{28,24},{5,1},{9,5},{13... | collective-permute-start | bytes 3080 | tf_op jit(solution)/shard_map/ppermute | solution.py:17
  408.1 37.7 %copy-start = (bf16[512,512]{1,0:T(8,128)(2,1)S(1)}, bf16[512,512]{1,0:T(8,128)(2,1)}, u32[]{:S(2)}) copy-start(bf16[512,512]{1,0:T(8,128)(2,1)} %add_convert_fusion.1) | copy-start | bytes 1572868
Sparse Core Ops, SparseCore 0:
  8.9 25.2 all-gather.6
  36.4 72.7 all-gather.12
  111.4 71.2 all-gather.10
  184.8 71.2 all-gather.8
  258.0 73.1 all-gather.14
  337.7 29.3 reduce-scatter.2
  369.2 22.5 all-gather.16
  414.6 31.1 reduce-scatter.4
where the time goes:
time: 455 us
  waiting for transfers between devices  386 us (85%)
  matrix products  25.4 us (6%)
  starting transfers between devices  15.4 us (3%)
  between operations  13.6 us (3%)
  other arithmetic  10.3 us (2%)
    all_gather x1, waiting for transfers between devices, per_device(): gathered_out = lax.all_gather(out_proj, 'sp', axis=2, tiled=True)  75.1 us
    all_gather x1, waiting for transfers between devices, per_device(): lax.all_gather(value_proj, 'sp', axis=1, tiled=True)  72.9 us
    all_gather x1, waiting for transfers between devices, per_device(): lax.all_gather(input_gate, 'sp', axis=1, tiled=True)  68.9 us
    all_gather x1, waiting for transfers between devices, per_device(): lax.all_gather(gate_proj, 'sp', axis=1, tiled=True)  66.4 us
    reduce_scatter x2, waiting for transfers between devices, per_device(): lax.psum_scatter(partials.astype(jnp.bfloat16), 'tp', scatter_dimension=1...  60.7 us
    all_gather x2, waiting for transfers between devices, per_device(): full_rows = lax.all_gather(current, 'tp', axis=1, tiled=True)  32.6 us
    dot_general x2, matrix products, per_device(): jnp.dot(gated, gathered_out[layer_index], preferred_element_type=jnp.floa...  12.7 us
    ppermute x3, starting transfers between devices, with_halo(): before = lax.ppermute(last, axis, up)  11.2 us
  transfers between devices with their start and end apart: 14, of which 10 were waited for; matrix products, arithmetic and copies ran while one was open for 3% of the time, Pallas kernels for 0%

commit v1 on v0

--- a/solution.py
+++ b/solution.py
@@ -22,7 +22,7 @@
 def per_device(stream, doc_ids, norm_gain, gate_proj, input_gate, value_proj, taps, out_proj):
     layers = gate_proj.shape[0]
     gathered_in = (
-        lax.all_gather(gate_proj, "sp", axis=1, tiled=True),
+        jnp.concatenate(lax.all_gather(gate_proj, "sp"), axis=1),
         lax.all_gather(input_gate, "sp", axis=1, tiled=True),
         lax.all_gather(value_proj, "sp", axis=1, tiled=True),
     )

time: 455 us -> 454 us (level)
    all_gather x1, waiting for transfers between devices: 75.1 us -> 70.5 us  [per_device(): gathered_out = lax.all_gather(out_proj, 'sp', axis=2, tiled=True)]
    slice x0 -> x1, local copies, waits for them, and re-layouts: none -> 4.6 us  [per_device(): gathered_in[0][layer_index]]
  transfers between devices with their start and end apart: 14 -> 14, of which waited for: 10 -> 10; matrix products, arithmetic and copies ran while one was open for 3% -> 4% of each run, Pallas kernels for 0% -> 0%
where the time goes in v1:
time: 454 us; the launch traced here: 453 us
  waiting for transfers between devices  385 us (85%)
  matrix products  23.8 us (5%)
  starting transfers between devices  15.5 us (3%)
  between operations  13.7 us (3%)
  other arithmetic  9.91 us (2%)
  local copies, waits for them, and re-layouts  5.25 us (1%)
    all_gather x1, waiting for transfers between devices, per_device(): lax.all_gather(value_proj, 'sp', axis=1, tiled=True)  72.8 us
    all_gather x1, waiting for transfers between devices, per_device(): gathered_out = lax.all_gather(out_proj, 'sp', axis=2, tiled=True)  70.5 us
    all_gather x1, waiting for transfers between devices, per_device(): lax.all_gather(input_gate, 'sp', axis=1, tiled=True)  69.7 us
    all_gather x1, waiting for transfers between devices, per_device(): lax.all_gather(gate_proj, 'sp')  66.4 us
    reduce_scatter x2, waiting for transfers between devices, per_device(): lax.psum_scatter(partials.astype(jnp.bfloat16), 'tp', scatter_dimension=1...  60.8 us
    all_gather x2, waiting for transfers between devices, per_device(): full_rows = lax.all_gather(current, 'tp', axis=1, tiled=True)  33.7 us
    dot_general x2, matrix products, per_device(): jnp.dot(gated, gathered_out[layer_index], preferred_element_type=jnp.floa...  12.4 us
    ppermute x3, starting transfers between devices, with_halo(): before = lax.ppermute(last, axis, up)  11.3 us
  transfers between devices with their start and end apart: 14, of which 10 were waited for; matrix products, arithmetic and copies ran while one was open for 4% of the time, Pallas kernels for 0%

profile of v1, /device:TPU:0, one launch (start us, length us, event | category | flops | bytes accessed | tf_op | source)
XLA Modules:
  0.0 453.5 jit_solution(3108508972889966958)
XLA Ops:
  6.5 0.0 copy-start.5
  6.5 0.0 copy-start.6
  6.5 0.0 all-gather.8.cloned.1.call-start
  6.5 0.7 all-gather.8.cloned.1.call-update
  7.3 0.0 all-gather.12.cloned.1.call-start
  7.3 0.7 all-gather.12.cloned.1.call-update
  8.0 0.0 all-gather.10.cloned.1.call-start
  8.1 0.7 all-gather.10.cloned.1.call-update
  8.7 0.0 all-gather.18.cloned.1.call-start
  8.8 0.5 all-gather.18.cloned.1.call-update
  9.3 0.0 all-gather.14.cloned.1.call-start
  9.4 0.5 all-gather.14.cloned.1.call-update
  9.9 0.0 reduce-scatter.3.cloned.1.call-start
  10.0 0.0 copy-done.5
  10.0 0.6 fusion.61
  10.6 5.5 %collective-permute-start = (s32[1]{0:T(128)}, s32[1]{0:T(128)}, u32[]{:S(2)}, u32[]{:S(2)}) collective-permute-start(s32[1]{0:T(128)} %get-tuple-element.23), channel_id=1, source_target_pairs={{0,4},{4,8},{8,12},{12,16},{16,20},{20,24},{24,28},{1,5},{5,9},{9,... | collective-permute-start | bytes 20 | tf_op jit(solution)/shard_map/ppermute | solution.py:16
  16.0 1.3 collective-permute-start.2
  17.3 0.0 copy-done.6
  17.3 0.0 copy-done.4
  17.4 0.0 collective-permute-done
  17.4 4.3 collective-permute-done.2
  21.6 1.4 pad_add_fusion
  23.1 0.1 slice_compare_fusion.1
  23.2 11.1 %all-gather.8.cloned.1.call-done = bf16[512,2048]{1,0:T(8,128)(2,1)} async-done(((bf16[512,512]{1,0:T(8,128)(2,1)}), bf16[512,2048]{1,0:T(8,128)(2,1)}) %all-gather.8.cloned.1.call-update) | async-done | bytes 2097168 | tf_op jit(solution)/shard_map/all_gather | solution.py:32
  34.2 0.0 copy-start.2
  34.2 2.2 fusion
  36.5 72.8 %all-gather.12.cloned.1.call-done = bf16[2,2048,512]{2,1,0:T(8,128)(2,1)} async-done(((bf16[2,256,512]{2,1,0:T(8,128)(2,1)}), bf16[2,2048,512]{2,1,0:T(8,128)(2,1)}) %all-gather.12.cloned.1.call-update) | async-done | bytes 4194320 | tf_op jit(solution)/shard_map/all_gather | solution.py:27
  109.2 0.0 copy-done.2
  109.2 3.9 fusion.14
  113.1 69.7 %all-gather.10.cloned.1.call-done = bf16[2,2048,512]{2,1,0:T(8,128)(2,1)} async-done(((bf16[2,256,512]{2,1,0:T(8,128)(2,1)}), bf16[2,2048,512]{2,1,0:T(8,128)(2,1)}) %all-gather.10.cloned.1.call-update) | async-done | bytes 4194320 | tf_op jit(solution)/shard_map/all_gather | solution.py:26
  182.7 3.2 fusion.27
  185.9 2.5 collective-permute-start.1
  188.4 1.3 collective-permute-start.3
  189.7 66.4 %all-gather.18.cloned.1.call-done = bf16[16,256,512]{2,1,0:T(8,128)(2,1)} async-done(((bf16[2,256,512]{2,1,0:T(8,128)(2,1)}), bf16[16,256,512]{2,1,0:T(8,128)(2,1)}) %all-gather.18.cloned.1.call-update) | async-done | bytes 4194320 | tf_op jit(solution)/shard_map/all_gather | solution.py:25
  256.1 4.6 %fusion.56 = (bf16[1,8,256,512]{3,2,0,1:T(8,128)(2,1)}, bf16[1,8,256,512]{3,2,0,1:T(8,128)(2,1)}) fusion(bf16[2,8,256,512]{3,2,0,1:T(8,128)(2,1)} %bitcast.57), kind=kLoop, calls=%fused_computation.74 | loop fusion | bytes 8388608 | tf_op jit(solution)/shard_map/slice | solution.py:36
  260.7 70.5 %all-gather.14.cloned.1.call-done = bf16[2,512,2048]{2,1,0:T(8,128)(2,1)} async-done(((bf16[2,512,256]{2,1,0:T(8,128)(2,1)}), bf16[2,512,2048]{2,1,0:T(8,128)(2,1)}) %all-gather.14.cloned.1.call-update) | async-done | bytes 4194320 | tf_op jit(solution)/shard_map/all_gather | solution.py:29
  331.2 0.0 collective-permute-done.1
  331.2 0.0 collective-permute-done.3
  331.2 6.2 %convolution_convert_fusion.1 = bf16[512,2048]{1,0:T(8,128)(2,1)} fusion(bf16[2,512,2048]{2,1,0:T(8,128)(2,1)} %all-gather.14.cloned.1.call-done, bf16[2048,512]{1,0:T(8,128)(2,1)} %bitcast.59, bf16[512,512]{1,0:T(8,128)(2,1)S(1)} %fusion.27, bf16[1,512]{1,0:T(2,128)(2,1)S(1)} %collective-permute-done.3, bf16[1,512]{1,0:T(2,128)(2,1)S(1)} %collective-permute-done.1, ...), kind=kOutput, calls=%fused_computation.11 | convolution fusion | flops 2157969408 | bytes 8932352 | tf_op jit(solution)/shard_map/dot_general | solution.py:56
  337.4 0.0 copy-start.1
  337.4 0.0 reduce-scatter.3.cloned.1.call-update
  337.4 0.0 all-gather.16.cloned.1.call-start
  337.5 29.5 %reduce-scatter.3.cloned.1.call-done = bf16[512,512]{1,0:T(8,128)(2,1)} async-done(((bf16[512,2048]{1,0:T(8,128)(2,1)}), bf16[512,512]{1,0:T(8,128)(2,1)}) %reduce-scatter.3.cloned.1.call-update) | async-done | bytes 524304 | tf_op jit(solution)/shard_map/reduce_scatter | solution.py:57
  366.9 0.0 copy-done.1
  366.9 2.0 add_convert_fusion.1
  368.9 0.0 all-gather.16.cloned.1.call-update
  368.9 0.0 reduce-scatter.5.cloned.1.call-start
  369.0 22.7 %all-gather.16.cloned.1.call-done = bf16[512,2048]{1,0:T(8,128)(2,1)} async-done(((bf16[512,512]{1,0:T(8,128)(2,1)}), bf16[512,2048]{1,0:T(8,128)(2,1)}) %all-gather.16.cloned.1.call-update) | async-done | bytes 2097168 | tf_op jit(solution)/shard_map/all_gather | solution.py:32
  391.6 0.0 copy-start.3
  391.6 2.2 fusion.3
  393.9 0.0 copy-done.3
  393.9 0.0 copy-start.7
  393.9 3.0 fusion.19
  396.9 0.0 copy-done.7
  396.9 1.3 fusion.26
  398.3 3.4 collective-permute-start.4
  401.7 1.3 collective-permute-start.5
  403.0 0.0 collective-permute-done.4
  403.0 4.2 collective-permute-done.5
  407.1 6.2 %convolution_convert_fusion = bf16[512,2048]{1,0:T(8,128)(2,1)} fusion(bf16[2,512,2048]{2,1,0:T(8,128)(2,1)} %all-gather.14.cloned.1.call-done, bf16[2048,512]{1,0:T(8,128)(2,1)} %bitcast.58, bf16[512,512]{1,0:T(8,128)(2,1)S(1)} %fusion.26, bf16[1,512]{1,0:T(2,128)(2,1)S(1)} %collective-permute-done.5, bf16[1,512]{1,0:T(2,128)(2,1)S(1)} %collective-permute-done.4, ...), kind=kOutput, calls=%fused_computation.10 | convolution fusion | flops 2157969408 | bytes 8932352 | tf_op jit(solution)/shard_map/dot_general | solution.py:56
  413.4 0.0 reduce-scatter.5.cloned.1.call-update
  413.4 31.3 %reduce-scatter.5.cloned.1.call-done = bf16[512,512]{1,0:T(8,128)(2,1)} async-done(((bf16[512,2048]{1,0:T(8,128)(2,1)}), bf16[512,512]{1,0:T(8,128)(2,1)}) %reduce-scatter.5.cloned.1.call-update) | async-done | bytes 524304 | tf_op jit(solution)/shard_map/reduce_scatter | solution.py:57
  444.7 0.0 copy-done
  444.7 2.0 add_convert_fusion
  (8 shorter events, 0.1 us)
Async XLA Ops:
  6.5 3.4 copy-start.5
  6.5 10.8 %copy-start.6 = (f32[2,3,512]{2,0,1:T(2,128)S(1)}, f32[2,3,512]{2,0,1:T(2,128)}, u32[]{:S(2)}) copy-start(f32[2,3,512]{2,0,1:T(2,128)} %param.14) | copy-start | bytes 36868
  6.5 10.8 %copy-start.4 = (f32[2,2048]{1,0:T(2,128)S(1)}, f32[2,2048]{1,0:T(2,128)}, u32[]{:S(2)}) copy-start(f32[2,2048]{1,0:T(2,128)} %param.10) | copy-start | bytes 49156
  6.5 27.7 %all-gather.8.cloned.1.call-start = ((), (), s32[]{:S(2)}) async-start(), calls=%async_computation.2 | async-start | bytes 2621440 | tf_op jit(solution)/shard_map/all_gather | solution.py:32
  7.3 101.9 %all-gather.12.cloned.1.call-start = ((), (), s32[]{:S(2)}) async-start(), calls=%async_computation.4 | async-start | bytes 4718592 | tf_op jit(solution)/shard_map/all_gather | solution.py:27
  8.0 174.7 %all-gather.10.cloned.1.call-start = ((), (), s32[]{:S(2)}) async-start(), calls=%async_computation.3 | async-start | bytes 4718592 | tf_op jit(solution)/shard_map/all_gather | solution.py:26
  8.7 247.3 %all-gather.18.cloned.1.call-start = ((), (), s32[]{:S(2)}) async-start(), calls=%async_computation.9 | async-start | bytes 4718592 | tf_op jit(solution)/shard_map/all_gather | solution.py:25
  9.3 321.9 %all-gather.14.cloned.1.call-start = ((), (), s32[]{:S(2)}) async-start(), calls=%async_computation.5 | async-start | bytes 4718592 | tf_op jit(solution)/shard_map/all_gather | solution.py:29
  9.9 357.0 %reduce-scatter.3.cloned.1.call-start = ((), (), s32[]{:S(2)}) async-start(), calls=%async_computation.6 | async-start | bytes 2621440 | tf_op jit(solution)/shard_map/reduce_scatter | solution.py:57
  10.6 6.8 %collective-permute-start = (s32[1]{0:T(128)}, s32[1]{0:T(128)}, u32[]{:S(2)}, u32[]{:S(2)}) collective-permute-start(s32[1]{0:T(128)} %get-tuple-element.23), channel_id=1, source_target_pairs={{0,4},{4,8},{8,12},{12,16},{16,20},{20,24},{24,28},{1,5},{5,9},{9,... | collective-permute-start | bytes 20 | tf_op jit(solution)/shard_map/ppermute | solution.py:16
  16.0 5.6 %collective-permute-start.2 = (s32[1]{0:T(128)}, s32[1]{0:T(128)}, u32[]{:S(2)}, u32[]{:S(2)}) collective-permute-start(s32[1]{0:T(128)} %get-tuple-element.24), channel_id=1, source_target_pairs={{4,0},{8,4},{12,8},{16,12},{20,16},{24,20},{28,24},{5,1},{9,5},{13... | collective-permute-start | bytes 20 | tf_op jit(solution)/shard_map/ppermute | solution.py:17
  34.2 75.0 %copy-start.2 = (bf16[512,2048]{1,0:T(8,128)(2,1)S(1)}, bf16[512,2048]{1,0:T(8,128)(2,1)}, u32[]{:S(2)}) copy-start(bf16[512,2048]{1,0:T(8,128)(2,1)} %all-gather.8.cloned.1.call-done) | copy-start | bytes 6291460
  185.9 145.3 %collective-permute-start.1 = (bf16[1,512]{1,0:T(2,128)(2,1)S(1)}, bf16[1,512]{1,0:T(2,128)(2,1)S(1)}, u32[]{:S(2)}, u32[]{:S(2)}) collective-permute-start(bf16[1,512]{1,0:T(2,128)(2,1)S(1)} %get-tuple-element.9), channel_id=1, source_target_pairs={{0,4},{4,8},{8,12},{12,16},{16,20},{20,24},{24,28},{1,5},{5,9},{9,... | collective-permute-start | bytes 3080 | tf_op jit(solution)/shard_map/ppermute | solution.py:16
  188.4 142.8 %collective-permute-start.3 = (bf16[1,512]{1,0:T(2,128)(2,1)S(1)}, bf16[1,512]{1,0:T(2,128)(2,1)S(1)}, u32[]{:S(2)}, u32[]{:S(2)}) collective-permute-start(bf16[1,512]{1,0:T(2,128)(2,1)S(1)} %get-tuple-element.10), channel_id=1, source_target_pairs={{4,0},{8,4},{12,8},{16,12},{20,16},{24,20},{28,24},{5,1},{9,5},{13... | collective-permute-start | bytes 3080 | tf_op jit(solution)/shard_map/ppermute | solution.py:17
  337.4 29.5 %copy-start.1 = (bf16[512,512]{1,0:T(8,128)(2,1)S(1)}, bf16[512,512]{1,0:T(8,128)(2,1)}, u32[]{:S(2)}) copy-start(bf16[512,512]{1,0:T(8,128)(2,1)} %param.8) | copy-start | bytes 1572868
  337.4 54.2 %all-gather.16.cloned.1.call-start = ((), (), s32[]{:S(2)}) async-start(), calls=%async_computation.7 | async-start | bytes 2621440 | tf_op jit(solution)/shard_map/all_gather | solution.py:32
  368.9 75.8 %reduce-scatter.5.cloned.1.call-start = ((), (), s32[]{:S(2)}) async-start(), calls=%async_computation.8 | async-start | bytes 2621440 | tf_op jit(solution)/shard_map/reduce_scatter | solution.py:57
  391.6 2.2 copy-start.3
  393.9 3.0 copy-start.7
  398.3 4.7 %collective-permute-start.4 = (bf16[1,512]{1,0:T(2,128)(2,1)S(1)}, bf16[1,512]{1,0:T(2,128)(2,1)S(1)}, u32[]{:S(2)}, u32[]{:S(2)}) collective-permute-start(bf16[1,512]{1,0:T(2,128)(2,1)S(1)} %get-tuple-element.7), channel_id=1, source_target_pairs={{0,4},{4,8},{8,12},{12,16},{16,20},{20,24},{24,28},{1,5},{5,9},{9,... | collective-permute-start | bytes 3080 | tf_op jit(solution)/shard_map/ppermute | solution.py:16
  401.7 5.5 %collective-permute-start.5 = (bf16[1,512]{1,0:T(2,128)(2,1)S(1)}, bf16[1,512]{1,0:T(2,128)(2,1)S(1)}, u32[]{:S(2)}, u32[]{:S(2)}) collective-permute-start(bf16[1,512]{1,0:T(2,128)(2,1)S(1)} %get-tuple-element.8), channel_id=1, source_target_pairs={{4,0},{8,4},{12,8},{16,12},{20,16},{24,20},{28,24},{5,1},{9,5},{13... | collective-permute-start | bytes 3080 | tf_op jit(solution)/shard_map/ppermute | solution.py:17
  413.4 31.3 %copy-start = (bf16[512,512]{1,0:T(8,128)(2,1)S(1)}, bf16[512,512]{1,0:T(8,128)(2,1)}, u32[]{:S(2)}) copy-start(bf16[512,512]{1,0:T(8,128)(2,1)} %add_convert_fusion.1) | copy-start | bytes 1572868
Sparse Core Ops, SparseCore 0:
  8.9 25.2 all-gather.7
  36.4 72.7 all-gather.11
  111.4 71.2 all-gather.9
  184.7 71.3 all-gather.17
  258.0 73.1 all-gather.13
  337.5 29.3 reduce-scatter.2
  369.1 22.5 all-gather.15
  413.5 31.1 reduce-scatter.4
